TPU v7x, 512 devices: a whole 4x4x16 slice. The times are simulated.
512 devices in a mesh: sp: 128 (over z, x, core), tp: 4 (over y).
Axes of the slice: x: 4, y: 4, z: 16, core: 2. Of those that a mesh axis runs over, the one named last changes fastest.
Arguments:
- queries: bfloat16 [32768, 1024], P('sp', 'tp'), may hold values from -6 to 6
- keys: bfloat16 [32768, 1024], P('sp', 'tp'), may hold values from -6 to 6
- values: bfloat16 [32768, 2048], P('sp', 'tp'), may hold values from -6 to 6
- gate_code: bfloat16 [32768, 32], P('sp'), may hold values from -5.5 to 5.5
- gate_up: bfloat16 [32, 1024], P(None, 'tp'), may hold values from -1 to 1
- gate_bias: float32 [1024], P('tp'), as said below
- gla_gain: float32 [256], replicated, may hold values from 0.1 to 1.9
- conv_input: bfloat16 [32768, 2048], P('sp', 'tp'), may hold values from -6 to 6
- conv_gate: bfloat16 [32768, 2048], P('sp', 'tp'), may hold values from -6 to 6
- conv_taps: float32 [3, 2048], P(None, 'tp'), may hold values from -3.5 to 3.5
- out_gla: bfloat16 [2048, 2048], P('tp', 'sp'), may hold values from -0.09375 to 0.09375
- out_conv: bfloat16 [2048, 2048], P('tp', 'sp'), may hold values from -0.09375 to 0.09375
Outputs:
- mixed: bfloat16 [32768, 2048], P(('sp', 'tp'))
Inputs may be any that keep to these rules, and one draw needn't show every extreme that they name: `gate_bias`: every bias is at least 1.5, so every decay per step lies strictly between 0 and 1.
All inputs are finite; a program needn't handle non-finite values.
Results may differ from a plain program's by a relative error of at most 0.028.
Values may be sent and summed in bfloat16 or wider, within the bound.
A program may use at most 64 MiB of HBM per device.

v0:
```python
import jax
import jax.numpy as jnp
from jax import lax
from jax.sharding import Mesh
from jax.sharding import PartitionSpec as P

KEY_WIDTH = 128
HEAD_V = 256
SEGMENT_LENGTH = 64
SP = ("sp_0", "sp_1", "sp_2")
SP_TP = ("sp_0", "sp_1", "sp_2", "tp")
softness_divisor = 16.0
epsilon = 1.0


def split_up(x, dim, count):
    dims = x.shape
    parts = x.reshape(*dims[:dim], count, dims[dim] // count, *dims[dim + 1 :])
    return jnp.moveaxis(parts, dim, 0)


def laid_out(parts, dim):
    parts = jnp.moveaxis(parts, 0, dim)
    dims = parts.shape
    return parts.reshape(*dims[:dim], dims[dim] * dims[dim + 1], *dims[dim + 2 :])


def turned_blocks(parts, axes, turns):
    inside = parts.shape[1:]
    out = parts.reshape(*(lax.axis_size(a) for a in axes), *inside)
    for k in turns:
        out = lax.all_to_all(out, axes[k], k, k, tiled=True)
    return out.reshape(-1, *inside)


def exchange_by_chip(x, groups, turns, split_dim, concat_dim):
    count = lax.axis_size(groups[0]) * lax.axis_size(groups[1])
    parts = split_up(x, split_dim, count)
    return laid_out(turned_blocks(parts, groups, turns), concat_dim)


def all_blocks(x, axes, turns):
    parts = x[None]
    for k in turns:
        parts = lax.all_gather(parts, axes[k], axis=0, tiled=True)
    current = [lax.axis_size(axes[k]) for k in reversed(turns)]
    parts = parts.reshape(*current, *x.shape)
    turned = sorted(range(len(turns)), key=lambda place: turns[len(turns) - 1 - place])
    return parts.transpose(*turned, *range(len(turns), parts.ndim)).reshape(-1, *x.shape)


def whole_of(x, axes, turns, dim):
    return laid_out(all_blocks(x, axes, turns), dim)


def for_sending(x):
    return jax.tree.map(lambda a: a.astype(jnp.bfloat16) if a.dtype == jnp.float32 else a, x)


def from_behind(x, axis, by):
    count = lax.axis_size(axis)
    pairs = [(i, i + by) for i in range(count) if 0 <= i + by < count]
    return lax.ppermute(x, axis, pairs)


def turned_gather(arrays, axis, dims):
    turned = [jnp.moveaxis(a, dim, 0) for a, dim in zip(arrays, dims)]
    both = jnp.concatenate([t.reshape(len(t), -1) for t in turned], axis=1)
    out, at, outs = (lax.all_gather(both, axis, axis=0, tiled=True), 0, [])
    for t, dim in zip(turned, dims):
        piece = out[:, at : at + t[0].size].reshape(-1, *t.shape[1:])
        outs.append(jnp.moveaxis(piece, 0, dim))
        at += t[0].size
    return tuple(outs)


def sent_and_summed(x, axis, dim):
    parts = split_up(x, dim, lax.axis_size(axis))
    arrived = lax.all_to_all(parts, axis, split_axis=0, concat_axis=0, tiled=True)
    return arrived.astype(jnp.float32).sum(axis=0)


def chain(earlier, latter):
    return (earlier[0] * latter[0], latter[0][..., None] * earlier[1] + latter[1])


def per_device(
    queries,
    keys,
    values,
    gate_code,
    gate_up,
    gate_bias,
    gla_gain,
    conv_input,
    conv_gate,
    conv_taps,
    out_gla,
    out_conv,
):
    row_count = queries.shape[0]
    segment_count = row_count // SEGMENT_LENGTH
    head_count = queries.shape[1] // KEY_WIDTH
    gate_score = jnp.dot(gate_code, gate_up, preferred_element_type=jnp.float32) + gate_bias
    decay_logarithm = (jax.nn.log_sigmoid(gate_score) / softness_divisor).reshape(
        segment_count, SEGMENT_LENGTH, head_count, KEY_WIDTH
    )
    inside = jnp.cumsum(decay_logarithm, axis=1)
    seg_total = inside[:, -1]
    key_blocks = keys.reshape(segment_count, SEGMENT_LENGTH, head_count, KEY_WIDTH)
    scaled_keys = (key_blocks * jnp.exp(seg_total[:, None] - inside)).astype(jnp.bfloat16)
    value_blocks = values.reshape(segment_count, SEGMENT_LENGTH, head_count, HEAD_V)
    update = jnp.einsum(
        "nshk,nshv->nhkv", scaled_keys, value_blocks, preferred_element_type=jnp.float32
    )
    through, local_state = lax.associative_scan(chain, (jnp.exp(seg_total), update), axis=0)
    device_decay = through[-1]
    device_state = local_state[-1]
    columns = exchange_by_chip(
        device_state[None].astype(jnp.bfloat16), (("sp_0", "sp_1"), "sp_2"), (1, 0), 3, 0
    ).astype(jnp.float32)
    decays = whole_of(device_decay[None], SP, (0, 1, 2), 0)
    running = lax.associative_scan(chain, (decays, columns), axis=0)[1]
    before = jnp.concatenate([jnp.zeros_like(running[:1]), running[:-1]], axis=0)
    incoming = lax.all_to_all(
        for_sending(before), SP, split_axis=0, concat_axis=3, tiled=True
    ).astype(before.dtype)[0]
    states = local_state + through[..., None] * incoming[None]
    query_blocks = queries.reshape(segment_count, SEGMENT_LENGTH, head_count, KEY_WIDTH)
    readout = jnp.einsum(
        "nshk,nhkv->nshv",
        query_blocks,
        states.astype(jnp.bfloat16),
        preferred_element_type=jnp.float32,
    )
    norm_scale = lax.rsqrt(jnp.mean(readout * readout, axis=-1, keepdims=True) + epsilon)
    gla_mix = (
        (readout * norm_scale * gla_gain)
        .astype(jnp.bfloat16)
        .reshape(row_count, head_count * HEAD_V)
    )
    reach_rows = conv_taps.shape[0] - 1
    earlier_rows = from_behind(conv_input[row_count - reach_rows :], SP, 1)
    extended = jnp.concatenate([earlier_rows, conv_input], axis=0)
    convolved = jnp.zeros(conv_input.shape, jnp.float32)
    for offset in range(reach_rows + 1):
        convolved = convolved + conv_taps[offset] * extended[offset : offset + row_count]
    conv_mix = (conv_gate * convolved).astype(jnp.bfloat16)
    wide_gla, wide_conv = turned_gather((out_gla, out_conv), SP, (1, 1))
    summed = jnp.dot(gla_mix, wide_gla, preferred_element_type=jnp.float32)
    mixed_rows = sent_and_summed(
        (summed + jnp.dot(conv_mix, wide_conv, preferred_element_type=jnp.float32)).astype(
            jnp.bfloat16
        ),
        "tp",
        0,
    )
    return mixed_rows.astype(jnp.bfloat16)


def solution(mesh):
    split = Mesh(mesh.devices.reshape(16, 4, 2, mesh.shape["tp"]), ("sp_0", "sp_1", "sp_2", "tp"))
    placed = (
        P(SP, "tp"),
        P(SP, "tp"),
        P(SP, "tp"),
        P(SP, None),
        P(None, "tp"),
        P("tp"),
        P(),
        P(SP, "tp"),
        P(SP, "tp"),
        P(None, "tp"),
        P("tp", SP),
        P("tp", SP),
    )
    return jax.shard_map(
        per_device, mesh=split, in_specs=placed, out_specs=P(SP_TP, None), check_vma=False
    )
```

profile of v0, /device:TPU:1, one launch (start us, length us, event | category | flops | bytes accessed | tf_op | source)
XLA Modules:
  0.0 189.0 jit_solution(4269959149335231402)
XLA Ops:
  6.5 1.4 pad_maximum_fusion.6
  8.0 1.1 fusion.12
  9.0 0.1 reshape.75
  9.2 0.1 fusion.36
  9.4 0.1 reshape.83
  9.6 0.2 multiply_convert_fusion.3
  9.8 0.3 fusion.14
  10.1 0.1 slice_add_fusion
  10.3 0.1 fusion.32
  10.4 0.1 fusion.31
  10.5 0.1 pad.73
  10.7 0.1 pad.74
  10.9 0.1 copy.69
  11.0 0.1 copy.70
  11.1 10.3 %all_to_all.24 = bf16[64,2,1,2,128,2]{4,5,0,3,2,1:T(2,128)(2,1)S(1)} all-to-all(bf16[64,2,1,2,128,2]{4,5,0,3,2,1:T(2,128)(2,1)S(1)} %copy.70), channel_id=1, replica_groups=mesh['sp_0'=16,'sp_1'=4,'sp_2'=2,'tp'=4] {'sp_2'}, dimensions={1} | all-to-all | bytes 262144 | tf_op jit(solution)/shard_map/all_to_all | solution.py:32
  21.4 0.7 copy.71
  22.2 12.9 %all-to-all-start.1 = ((bf16[64,2,1,2,128,2]{4,5,1,3,2,0:T(2,128)(2,1)}), bf16[64,2,1,2,128,2]{4,5,1,3,2,0:T(2,128)(2,1)S(1)}, u32[]{:S(2)}, u32[]{:S(2)}) async-start(bf16[64,2,1,2,128,2]{4,5,1,3,2,0:T(2,128)(2,1)} %copy.71), calls=%async_computation.1 | async-start | bytes 262144 | tf_op jit(solution)/shard_map/all_to_all | solution.py:32
  35.2 25.6 %all-gather = f32[16,2,128]{2,1,0:T(2,128)S(1)} all-gather(f32[1,2,128]{2,1,0:T(2,128)S(1)} %slice_add_fusion.4), channel_id=2, replica_groups=mesh['sp_0'=16,'sp_1'=4,'sp_2'=2,'tp'=4] {'sp_0'}, dimensions={0}, use_global_device_ids=true | all-gather | bytes 17408 | tf_op jit(solution)/shard_map/all_gather | solution.py:45
  60.8 10.3 %all-gather.1 = f32[64,2,128]{2,1,0:T(2,128)S(1)} all-gather(f32[16,2,128]{2,1,0:T(2,128)S(1)} %all-gather), channel_id=3, replica_groups=mesh['sp_0'=16,'sp_1'=4,'sp_2'=2,'tp'=4] {'sp_1'}, dimensions={0}, use_global_device_ids=true | all-gather | bytes 81920 | tf_op jit(solution)/shard_map/all_gather | solution.py:45
  71.1 9.7 %all-gather.2 = f32[128,2,128]{2,1,0:T(2,128)S(1)} all-gather(f32[64,2,128]{2,1,0:T(2,128)S(1)} %all-gather.1), channel_id=4, replica_groups=mesh['sp_0'=16,'sp_1'=4,'sp_2'=2,'tp'=4] {'sp_2'}, dimensions={0}, use_global_device_ids=true | all-gather | bytes 196608 | tf_op jit(solution)/shard_map/all_gather | solution.py:45
  80.8 0.1 copy.74
  81.4 0.2 copy.73
  81.6 0.1 slice.267
  81.7 0.1 slice.268
  81.8 0.1 slice.273
  81.9 0.1 slice.274
  82.4 0.1 slice.292
  82.6 0.1 slice.298
  82.6 0.1 slice.306
  82.9 0.1 slice.312
  83.0 0.1 slice.314
  84.2 0.1 copy.80
  84.3 0.8 concatenate.41.clone
  85.1 13.7 %all-to-all-start.2 = ((bf16[128,2,128,2]{2,3,1,0:T(2,128)(2,1)}), bf16[128,2,128,2]{2,3,1,0:T(2,128)(2,1)S(1)}, u32[]{:S(2)}, u32[]{:S(2)}) async-start(bf16[128,2,128,2]{2,3,1,0:T(2,128)(2,1)} %concatenate.41.clone), calls=%async_computation.2 | async-start | bytes 262144 | tf_op jit(solution)/shard_map/all_to_all | solution.py:125
  98.8 3.5 %collective-permute-start = (bf16[2,512]{1,0:T(2,128)(2,1)S(1)}, bf16[2,512]{1,0:T(2,128)(2,1)S(1)}, u32[]{:S(2)}, u32[]{:S(2)}) collective-permute-start(bf16[2,512]{1,0:T(2,128)(2,1)S(1)} %slice.318), channel_id=1, source_target_pairs={{0,4},{4,8},{8,12},{12,16},{16,20},{20,24},{24,28},{28,32},{32,36}... | collective-permute-start | bytes 6152 | tf_op jit(solution)/shard_map/ppermute | solution.py:63
  102.5 12.7 %all-to-all-done.2 = bf16[128,2,128,2]{2,3,1,0:T(2,128)(2,1)S(1)} async-done(((bf16[128,2,128,2]{2,3,1,0:T(2,128)(2,1)}), bf16[128,2,128,2]{2,3,1,0:T(2,128)(2,1)S(1)}, u32[]{:S(2)}, u32[]{:S(2)}) %all-to-all-start.2) | async-done | bytes 131104 | tf_op jit(solution)/shard_map/all_to_all | solution.py:125
  115.1 0.1 convert_bitcast_fusion
  115.2 0.1 copy.76
  115.3 0.1 copy.77
  115.5 0.5 multiply_reduce_fusion
  115.9 0.1 multiply_convert_fusion.1
  116.1 0.3 copy.79
  116.4 42.7 %all-gather.5.cloned.1.call-done = bf16[2048,1024]{1,0:T(8,128)(2,1)} async-done(((bf16[16,1024]{1,0:T(8,128)(2,1)}), bf16[2048,1024]{1,0:T(8,128)(2,1)}) %all-gather.5.cloned.1.call-update) | async-done | bytes 4194320 | tf_op jit(solution)/shard_map/all_gather | solution.py:69
  159.1 2.5 %fusion.2 = f32[256,2048]{1,0:T(8,128)S(1)} fusion(bf16[256,512]{1,0:T(8,128)(2,1)S(1)} %bitcast.45, bf16[2048,1024]{1,0:T(8,128)(2,1)} %all-gather.5.cloned.1.call-done), kind=kOutput, calls=%fused_computation.3 | convolution fusion | flops 536870912 | bytes 4456448 | tf_op jit(solution)/shard_map/dot_general | solution.py:150
  161.6 0.3 copy-done.1
  162.0 0.9 fusion
  162.8 18.4 %all_to_all.25 = bf16[4,64,2048]{2,1,0:T(8,128)(2,1)S(1)} all-to-all(bf16[4,64,2048]{2,1,0:T(8,128)(2,1)S(1)} %bitcast.46), channel_id=1, replica_groups=mesh['sp_0'=16,'sp_1'=4,'sp_2'=2,'tp'=4] {'tp'}, dimensions={0} | all-to-all | bytes 2097152 | tf_op jit(solution)/shard_map/all_to_all | solution.py:79
  181.3 0.9 reduce_sum.22
  (117 shorter events, 2.2 us)
Async XLA Ops:
  6.5 1.4 copy-start
  6.5 2.8 %copy-start.3 = (bf16[256,256]{1,0:T(8,128)(2,1)S(1)}, bf16[256,256]{1,0:T(8,128)(2,1)}, u32[]{:S(2)}) copy-start(bf16[256,256]{1,0:T(8,128)(2,1)} %param.13) | copy-start | bytes 393220
  6.5 3.0 %copy-start.2 = (bf16[256,512]{1,0:T(8,128)(2,1)S(1)}, bf16[256,512]{1,0:T(8,128)(2,1)}, u32[]{:S(2)}) copy-start(bf16[256,512]{1,0:T(8,128)(2,1)} %param.14) | copy-start | bytes 786436
  6.5 152.6 %all-gather.5.cloned.1.call-start = ((), (), s32[]{:S(2)}) async-start(), calls=%async_computation.4 | async-start | bytes 4227072 | tf_op jit(solution)/shard_map/all_gather | solution.py:69
  22.2 59.1 %all-to-all-start.1 = ((bf16[64,2,1,2,128,2]{4,5,1,3,2,0:T(2,128)(2,1)}), bf16[64,2,1,2,128,2]{4,5,1,3,2,0:T(2,128)(2,1)S(1)}, u32[]{:S(2)}, u32[]{:S(2)}) async-start(bf16[64,2,1,2,128,2]{4,5,1,3,2,0:T(2,128)(2,1)} %copy.71), calls=%async_computation.1 | async-start | bytes 262144 | tf_op jit(solution)/shard_map/all_to_all | solution.py:32
  83.8 15.0 %copy-start.7 = (bf16[256,512]{1,0:T(8,128)(2,1)S(1)}, bf16[256,512]{1,0:T(8,128)(2,1)}, u32[]{:S(2)}) copy-start(bf16[256,512]{1,0:T(8,128)(2,1)} %param.19) | copy-start | bytes 786436
  83.8 18.6 %copy-start.4 = (bf16[256,256]{1,0:T(8,128)(2,1)S(1)}, bf16[256,256]{1,0:T(8,128)(2,1)}, u32[]{:S(2)}) copy-start(bf16[256,256]{1,0:T(8,128)(2,1)} %param.12) | copy-start | bytes 393220
  83.8 18.6 %copy-start.5 = (f32[3,512]{1,0:T(4,128)S(1)}, f32[3,512]{1,0:T(4,128)}, u32[]{:S(2)}) copy-start(f32[3,512]{1,0:T(4,128)} %param.21) | copy-start | bytes 18436
  85.1 30.0 %all-to-all-start.2 = ((bf16[128,2,128,2]{2,3,1,0:T(2,128)(2,1)}), bf16[128,2,128,2]{2,3,1,0:T(2,128)(2,1)S(1)}, u32[]{:S(2)}, u32[]{:S(2)}) async-start(bf16[128,2,128,2]{2,3,1,0:T(2,128)(2,1)} %concatenate.41.clone), calls=%async_computation.2 | async-start | bytes 262144 | tf_op jit(solution)/shard_map/all_to_all | solution.py:125
  98.8 62.8 %collective-permute-start = (bf16[2,512]{1,0:T(2,128)(2,1)S(1)}, bf16[2,512]{1,0:T(2,128)(2,1)S(1)}, u32[]{:S(2)}, u32[]{:S(2)}) collective-permute-start(bf16[2,512]{1,0:T(2,128)(2,1)S(1)} %slice.318), channel_id=1, source_target_pairs={{0,4},{4,8},{8,12},{12,16},{16,20},{20,24},{24,28},{28,32},{32,36}... | collective-permute-start | bytes 6152 | tf_op jit(solution)/shard_map/ppermute | solution.py:63
  115.2 0.7 copy-start.6
  159.1 2.8 %copy-start.1 = (bf16[2048,1024]{1,0:T(8,128)(2,1)S(1)}, bf16[2048,1024]{1,0:T(8,128)(2,1)}, u32[]{:S(2)}) copy-start(bf16[2048,1024]{1,0:T(8,128)(2,1)} %all-gather.5.cloned.1.call-done) | copy-start | bytes 12582916
  159.1 2.8 %copy-start.8 = (bf16[256,512]{1,0:T(8,128)(2,1)S(1)}, bf16[256,512]{1,0:T(8,128)(2,1)}, u32[]{:S(2)}) copy-start(bf16[256,512]{1,0:T(8,128)(2,1)} %param.20) | copy-start | bytes 786436
Sparse Core Ops, SparseCore 0:
  10.5 148.5 all-gather.4
where the time goes:
time: 189 us
  blocking collectives  74.3 us (39%)
  waiting for transfers between devices  55.4 us (29%)
  starting transfers between devices  30.2 us (16%)
  between operations  14.3 us (8%)
  local copies, waits for them, and re-layouts  5.91 us (3%)
  matrix products  5.23 us (3%)
  other arithmetic  3.7 us (2%)
    all_gather x3, blocking collectives, all_blocks(): parts = lax.all_gather(parts, axes[k], axis=0, tiled=True)  45.6 us
    all_gather x1, waiting for transfers between devices, turned_gather(): out, at, outs = (lax.all_gather(both, axis, axis=0, tiled=True), 0, [])  42.7 us
    all_to_all x1, blocking collectives, sent_and_summed(): lax.all_to_all(parts, axis, split_axis=0, concat_axis=0, tiled=True)  18.4 us
    all_to_all x1, starting transfers between devices, per_device(): lax.all_to_all(for_sending(before), SP, split_axis=0, concat_axis=3, tile...  13.7 us
    all_to_all x1, starting transfers between devices, turned_blocks(): out = lax.all_to_all(out, axes[k], k, k, tiled=True)  12.9 us
    all_to_all x1, waiting for transfers between devices, per_device(): lax.all_to_all(for_sending(before), SP, split_axis=0, concat_axis=3, tile...  12.7 us
    all_to_all x1, blocking collectives, turned_blocks(): out = lax.all_to_all(out, axes[k], k, k, tiled=True)  10.3 us
  transfers between devices with their start and end apart: 4, of which 2 were waited for; matrix products, arithmetic and copies ran while one was open for 6% of the time, Pallas kernels for 0%

commit v1 on v0

--- a/solution.py
+++ b/solution.py
@@ -42,7 +42,11 @@
 def all_blocks(x, axes, turns):
     parts = x[None]
     for k in turns:
-        parts = lax.all_gather(parts, axes[k], axis=0, tiled=True)
+        local_block = axes[k]
+        windows = []
+        for _ in range(lax.axis_size(local_block)):
+            windows.append(parts)
+        parts = jnp.concatenate(lax.all_to_all(jnp.stack(windows, 0), local_block, 0, 0), 0)
     current = [lax.axis_size(axes[k]) for k in reversed(turns)]
     parts = parts.reshape(*current, *x.shape)
     turned = sorted(range(len(turns)), key=lambda place: turns[len(turns) - 1 - place])

time: 189 us -> 204 us (1.079)
  waiting for transfers between devices: 55.4 us -> 106 us
  blocking collectives: 74.3 us -> 23.7 us
  starting transfers between devices: 30.2 us -> 41.8 us
  local copies, waits for them, and re-layouts: 5.91 us -> 8.51 us
    all_gather x3 -> x0, blocking collectives: 45.6 us -> none  [all_blocks(): parts = lax.all_gather(parts, axes[k], axis=0, tiled=True)]
    all_gather x1, waiting for transfers between devices: 42.7 us -> 66.1 us  [turned_gather(): out, at, outs = (lax.all_gather(both, axis, axis=0, tiled=True), 0, [])]
    all_to_all x0 -> x2, starting transfers between devices: none -> 19.7 us  [all_blocks(): lax.all_to_all(jnp.stack(windows, 0), local_block, 0, 0)]
    all_to_all x1 -> x2, waiting for transfers between devices: 0.01 us -> 16.2 us  [turned_blocks(): out = lax.all_to_all(out, axes[k], k, k, tiled=True)]
    all_to_all x0 -> x2, waiting for transfers between devices: none -> 11.3 us  [all_blocks(): lax.all_to_all(jnp.stack(windows, 0), local_block, 0, 0)]
    all_to_all x1, starting transfers between devices: 13.7 us -> 8.45 us  [per_device(): lax.all_to_all(for_sending(before), SP, split_axis=0, concat_axis=3, tile...]
    all_to_all x1, blocking collectives: 10.3 us -> 5.27 us  [all_blocks(): lax.all_to_all(jnp.stack(windows, 0), local_block, 0, 0)]
    all_to_all x1 -> x2, starting transfers between devices: 12.9 us -> 10.1 us  [turned_blocks(): out = lax.all_to_all(out, axes[k], k, k, tiled=True)]
  transfers between devices with their start and end apart: 4 -> 7, of which waited for: 2 -> 6; matrix products, arithmetic and copies ran while one was open for 6% -> 6% of each run, Pallas kernels for 0% -> 0%
where the time goes in v1:
time: 204 us
  waiting for transfers between devices  106 us (52%)
  starting transfers between devices  41.8 us (20%)
  blocking collectives  23.7 us (12%)
  between operations  14.3 us (7%)
  local copies, waits for them, and re-layouts  8.51 us (4%)
  matrix products  5.22 us (3%)
  other arithmetic  3.66 us (2%)
    all_gather x1, waiting for transfers between devices, turned_gather(): out, at, outs = (lax.all_gather(both, axis, axis=0, tiled=True), 0, [])  66.1 us
    all_to_all x2, starting transfers between devices, all_blocks(): lax.all_to_all(jnp.stack(windows, 0), local_block, 0, 0)  19.7 us
    all_to_all x1, blocking collectives, sent_and_summed(): lax.all_to_all(parts, axis, split_axis=0, concat_axis=0, tiled=True)  18.4 us
    all_to_all x2, waiting for transfers between devices, turned_blocks(): out = lax.all_to_all(out, axes[k], k, k, tiled=True)  16.2 us
    all_to_all x1, waiting for transfers between devices, per_device(): lax.all_to_all(for_sending(before), SP, split_axis=0, concat_axis=3, tile...  12.6 us
    all_to_all x2, waiting for transfers between devices, all_blocks(): lax.all_to_all(jnp.stack(windows, 0), local_block, 0, 0)  11.3 us
    all_to_all x2, starting transfers between devices, turned_blocks(): out = lax.all_to_all(out, axes[k], k, k, tiled=True)  10.1 us
    all_to_all x1, starting transfers between devices, per_device(): lax.all_to_all(for_sending(before), SP, split_axis=0, concat_axis=3, tile...  8.45 us
  transfers between devices with their start and end apart: 7, of which 6 were waited for; matrix products, arithmetic and copies ran while one was open for 6% of the time, Pallas kernels for 0%

profile of v1, /device:TPU:1, one launch (start us, length us, event | category | flops | bytes accessed | tf_op | source)
XLA Modules:
  0.0 203.5 jit_solution(1644748539338391772)
XLA Ops:
  6.5 0.7 copy-done
  7.3 1.1 fusion.12
  8.3 0.1 reshape.79
  8.5 0.1 fusion.36
  8.7 0.6 stack.9
  9.3 15.7 %all-to-all-start.2 = ((f32[16,1,1,2,128]{4,3,2,1,0:T(2,128)}), f32[16,1,1,2,128]{4,3,2,1,0:T(2,128)S(1)}, u32[]{:S(2)}, u32[]{:S(2)}) async-start(f32[16,1,1,2,128]{4,3,2,1,0:T(2,128)} %stack.9), calls=%async_computation.2 | async-start | bytes 32768 | tf_op jit(solution)/shard_map/all_to_all | solution.py:49
  25.1 1.3 pad_maximum_fusion.7
  26.5 0.1 reshape.86
  26.7 0.2 multiply_convert_fusion.3
  26.9 0.3 fusion.14
  27.3 0.1 slice_add_fusion
  27.4 0.1 fusion.32
  27.5 0.1 fusion.31
  27.7 0.1 pad.73
  27.8 0.1 pad.74
  28.0 0.1 copy.89
  28.1 0.8 copy.90
  28.9 7.6 %all-to-all-done.2 = f32[16,1,1,2,128]{4,3,2,1,0:T(2,128)S(1)} async-done(((f32[16,1,1,2,128]{4,3,2,1,0:T(2,128)}), f32[16,1,1,2,128]{4,3,2,1,0:T(2,128)S(1)}, u32[]{:S(2)}, u32[]{:S(2)}) %all-to-all-start.2) | async-done | bytes 16416 | tf_op jit(solution)/shard_map/all_to_all | solution.py:49
  36.5 5.4 %all-to-all-start = ((bf16[64,2,1,2,128,2]{4,5,0,3,2,1:T(2,128)(2,1)}), bf16[64,2,1,2,128,2]{4,5,0,3,2,1:T(2,128)(2,1)S(1)}, u32[]{:S(2)}, u32[]{:S(2)}) async-start(bf16[64,2,1,2,128,2]{4,5,0,3,2,1:T(2,128)(2,1)} %copy.90), calls=%async_computation | async-start | bytes 262144 | tf_op jit(solution)/shard_map/all_to_all | solution.py:32
  41.9 1.1 all-to-all-done
  43.0 0.6 stack.10
  43.6 4.0 %all-to-all-start.3 = ((f32[4,16,1,2,128]{4,1,3,2,0:T(8,128)}), f32[4,16,1,2,128]{4,1,3,2,0:T(8,128)S(1)}, u32[]{:S(2)}, u32[]{:S(2)}) async-start(f32[4,16,1,2,128]{4,1,3,2,0:T(8,128)} %stack.10), calls=%async_computation.3 | async-start | bytes 131072 | tf_op jit(solution)/shard_map/all_to_all | solution.py:49
  47.6 0.7 copy.91
  48.4 3.7 %all-to-all-done.3 = f32[4,16,1,2,128]{4,1,3,2,0:T(8,128)S(1)} async-done(((f32[4,16,1,2,128]{4,1,3,2,0:T(8,128)}), f32[4,16,1,2,128]{4,1,3,2,0:T(8,128)S(1)}, u32[]{:S(2)}, u32[]{:S(2)}) %all-to-all-start.3) | async-done | bytes 65568 | tf_op jit(solution)/shard_map/all_to_all | solution.py:49
  52.1 5.3 %all_to_all.39 = f32[2,64,1,2,128]{4,1,3,2,0:T(8,128)S(1)} all-to-all(f32[2,64,1,2,128]{4,1,3,2,0:T(8,128)S(1)} %pad_maximum_fusion.3), channel_id=1, replica_groups=mesh['sp_0'=16,'sp_1'=4,'sp_2'=2,'tp'=4] {'sp_2'}, dimensions={0} | all-to-all | bytes 262144 | tf_op jit(solution)/shard_map/all_to_all | solution.py:49
  57.4 4.6 %all-to-all-start.1 = ((bf16[64,2,1,2,128,2]{4,5,1,3,2,0:T(2,128)(2,1)}), bf16[64,2,1,2,128,2]{4,5,1,3,2,0:T(2,128)(2,1)S(1)}, u32[]{:S(2)}, u32[]{:S(2)}) async-start(bf16[64,2,1,2,128,2]{4,5,1,3,2,0:T(2,128)(2,1)} %copy.91), calls=%async_computation.1 | async-start | bytes 262144 | tf_op jit(solution)/shard_map/all_to_all | solution.py:32
  62.0 0.1 copy.96
  62.6 15.1 %all-to-all-done.1 = bf16[64,2,1,2,128,2]{4,5,1,3,2,0:T(2,128)(2,1)S(1)} async-done(((bf16[64,2,1,2,128,2]{4,5,1,3,2,0:T(2,128)(2,1)}), bf16[64,2,1,2,128,2]{4,5,1,3,2,0:T(2,128)(2,1)S(1)}, u32[]{:S(2)}, u32[]{:S(2)}) %all-to-all-start.1) | async-done | bytes 131104 | tf_op jit(solution)/shard_map/all_to_all | solution.py:32
  77.7 0.2 copy.93
  78.0 0.1 slice.271
  79.4 0.1 slice.317
  80.6 0.1 copy.102
  80.7 0.8 concatenate.41.clone
  81.5 8.5 %all-to-all-start.5 = ((bf16[128,2,128,2]{2,3,1,0:T(2,128)(2,1)}), bf16[128,2,128,2]{2,3,1,0:T(2,128)(2,1)S(1)}, u32[]{:S(2)}, u32[]{:S(2)}) async-start(bf16[128,2,128,2]{2,3,1,0:T(2,128)(2,1)} %concatenate.41.clone), calls=%async_computation.5 | async-start | bytes 262144 | tf_op jit(solution)/shard_map/all_to_all | solution.py:129
  89.9 3.5 %collective-permute-start = (bf16[2,512]{1,0:T(2,128)(2,1)S(1)}, bf16[2,512]{1,0:T(2,128)(2,1)S(1)}, u32[]{:S(2)}, u32[]{:S(2)}) collective-permute-start(bf16[2,512]{1,0:T(2,128)(2,1)S(1)} %slice.321), channel_id=1, source_target_pairs={{0,4},{4,8},{8,12},{12,16},{16,20},{20,24},{24,28},{28,32},{32,36}... | collective-permute-start | bytes 6152 | tf_op jit(solution)/shard_map/ppermute | solution.py:67
  93.6 12.6 %all-to-all-done.5 = bf16[128,2,128,2]{2,3,1,0:T(2,128)(2,1)S(1)} async-done(((bf16[128,2,128,2]{2,3,1,0:T(2,128)(2,1)}), bf16[128,2,128,2]{2,3,1,0:T(2,128)(2,1)S(1)}, u32[]{:S(2)}, u32[]{:S(2)}) %all-to-all-start.5) | async-done | bytes 131104 | tf_op jit(solution)/shard_map/all_to_all | solution.py:129
  106.2 0.1 convert_bitcast_fusion
  106.3 0.1 copy.98
  106.4 0.1 copy.99
  106.5 0.5 multiply_reduce_fusion
  107.0 0.1 multiply_convert_fusion.1
  107.2 0.3 copy.101
  107.5 66.1 %all-gather.2.cloned.1.call-done = bf16[2048,1024]{1,0:T(8,128)(2,1)} async-done(((bf16[16,1024]{1,0:T(8,128)(2,1)}), bf16[2048,1024]{1,0:T(8,128)(2,1)}) %all-gather.2.cloned.1.call-update) | async-done | bytes 4194320 | tf_op jit(solution)/shard_map/all_gather | solution.py:73
  173.6 2.5 %fusion.2 = f32[256,2048]{1,0:T(8,128)S(1)} fusion(bf16[256,512]{1,0:T(8,128)(2,1)S(1)} %bitcast.49, bf16[2048,1024]{1,0:T(8,128)(2,1)} %all-gather.2.cloned.1.call-done), kind=kOutput, calls=%fused_computation.3 | convolution fusion | flops 536870912 | bytes 4456448 | tf_op jit(solution)/shard_map/dot_general | solution.py:154
  176.1 0.3 copy-done.1
  176.4 0.9 fusion
  177.3 18.4 %all_to_all.40 = bf16[4,64,2048]{2,1,0:T(8,128)(2,1)S(1)} all-to-all(bf16[4,64,2048]{2,1,0:T(8,128)(2,1)S(1)} %bitcast.50), channel_id=1, replica_groups=mesh['sp_0'=16,'sp_1'=4,'sp_2'=2,'tp'=4] {'tp'}, dimensions={0} | all-to-all | bytes 2097152 | tf_op jit(solution)/shard_map/all_to_all | solution.py:83
  195.7 0.9 reduce_sum.22
  (125 shorter events, 2.8 us)
Async XLA Ops:
  6.5 0.7 copy-start
  6.5 19.9 %copy-start.3 = (bf16[256,256]{1,0:T(8,128)(2,1)S(1)}, bf16[256,256]{1,0:T(8,128)(2,1)}, u32[]{:S(2)}) copy-start(bf16[256,256]{1,0:T(8,128)(2,1)} %param.13) | copy-start | bytes 393220
  6.5 20.1 %copy-start.2 = (bf16[256,512]{1,0:T(8,128)(2,1)S(1)}, bf16[256,512]{1,0:T(8,128)(2,1)}, u32[]{:S(2)}) copy-start(bf16[256,512]{1,0:T(8,128)(2,1)} %param.14) | copy-start | bytes 786436
  9.3 27.1 %all-to-all-start.2 = ((f32[16,1,1,2,128]{4,3,2,1,0:T(2,128)}), f32[16,1,1,2,128]{4,3,2,1,0:T(2,128)S(1)}, u32[]{:S(2)}, u32[]{:S(2)}) async-start(f32[16,1,1,2,128]{4,3,2,1,0:T(2,128)} %stack.9), calls=%async_computation.2 | async-start | bytes 32768 | tf_op jit(solution)/shard_map/all_to_all | solution.py:49
  25.1 148.5 %all-gather.2.cloned.1.call-start = ((), (), s32[]{:S(2)}) async-start(), calls=%async_computation.7 | async-start | bytes 4227072 | tf_op jit(solution)/shard_map/all_gather | solution.py:73
  36.5 6.6 %all-to-all-start = ((bf16[64,2,1,2,128,2]{4,5,0,3,2,1:T(2,128)(2,1)}), bf16[64,2,1,2,128,2]{4,5,0,3,2,1:T(2,128)(2,1)S(1)}, u32[]{:S(2)}, u32[]{:S(2)}) async-start(bf16[64,2,1,2,128,2]{4,5,0,3,2,1:T(2,128)(2,1)} %copy.90), calls=%async_computation | async-start | bytes 262144 | tf_op jit(solution)/shard_map/all_to_all | solution.py:32
  43.6 8.5 %all-to-all-start.3 = ((f32[4,16,1,2,128]{4,1,3,2,0:T(8,128)}), f32[4,16,1,2,128]{4,1,3,2,0:T(8,128)S(1)}, u32[]{:S(2)}, u32[]{:S(2)}) async-start(f32[4,16,1,2,128]{4,1,3,2,0:T(8,128)} %stack.10), calls=%async_computation.3 | async-start | bytes 131072 | tf_op jit(solution)/shard_map/all_to_all | solution.py:49
  57.4 20.3 %all-to-all-start.1 = ((bf16[64,2,1,2,128,2]{4,5,1,3,2,0:T(2,128)(2,1)}), bf16[64,2,1,2,128,2]{4,5,1,3,2,0:T(2,128)(2,1)S(1)}, u32[]{:S(2)}, u32[]{:S(2)}) async-start(bf16[64,2,1,2,128,2]{4,5,1,3,2,0:T(2,128)(2,1)} %copy.91), calls=%async_computation.1 | async-start | bytes 262144 | tf_op jit(solution)/shard_map/all_to_all | solution.py:32
  80.1 9.8 %copy-start.7 = (bf16[256,512]{1,0:T(8,128)(2,1)S(1)}, bf16[256,512]{1,0:T(8,128)(2,1)}, u32[]{:S(2)}) copy-start(bf16[256,512]{1,0:T(8,128)(2,1)} %param.19) | copy-start | bytes 786436
  80.1 13.4 %copy-start.4 = (bf16[256,256]{1,0:T(8,128)(2,1)S(1)}, bf16[256,256]{1,0:T(8,128)(2,1)}, u32[]{:S(2)}) copy-start(bf16[256,256]{1,0:T(8,128)(2,1)} %param.12) | copy-start | bytes 393220
  80.2 13.4 %copy-start.5 = (f32[3,512]{1,0:T(4,128)S(1)}, f32[3,512]{1,0:T(4,128)}, u32[]{:S(2)}) copy-start(f32[3,512]{1,0:T(4,128)} %param.21) | copy-start | bytes 18436
  81.5 24.7 %all-to-all-start.5 = ((bf16[128,2,128,2]{2,3,1,0:T(2,128)(2,1)}), bf16[128,2,128,2]{2,3,1,0:T(2,128)(2,1)S(1)}, u32[]{:S(2)}, u32[]{:S(2)}) async-start(bf16[128,2,128,2]{2,3,1,0:T(2,128)(2,1)} %concatenate.41.clone), calls=%async_computation.5 | async-start | bytes 262144 | tf_op jit(solution)/shard_map/all_to_all | solution.py:129
  89.9 86.1 %collective-permute-start = (bf16[2,512]{1,0:T(2,128)(2,1)S(1)}, bf16[2,512]{1,0:T(2,128)(2,1)S(1)}, u32[]{:S(2)}, u32[]{:S(2)}) collective-permute-start(bf16[2,512]{1,0:T(2,128)(2,1)S(1)} %slice.321), channel_id=1, source_target_pairs={{0,4},{4,8},{8,12},{12,16},{16,20},{20,24},{24,28},{28,32},{32,36}... | collective-permute-start | bytes 6152 | tf_op jit(solution)/shard_map/ppermute | solution.py:67
  106.3 0.7 copy-start.6
  173.6 2.8 %copy-start.1 = (bf16[2048,1024]{1,0:T(8,128)(2,1)S(1)}, bf16[2048,1024]{1,0:T(8,128)(2,1)}, u32[]{:S(2)}) copy-start(bf16[2048,1024]{1,0:T(8,128)(2,1)} %all-gather.2.cloned.1.call-done) | copy-start | bytes 12582916
  173.6 2.8 %copy-start.8 = (bf16[256,512]{1,0:T(8,128)(2,1)S(1)}, bf16[256,512]{1,0:T(8,128)(2,1)}, u32[]{:S(2)}) copy-start(bf16[256,512]{1,0:T(8,128)(2,1)} %param.20) | copy-start | bytes 786436
Sparse Core Ops, SparseCore 0:
  29.0 144.5 all-gather.1
